TPU v7x, 256 devices: a whole 4x4x8 slice. The times are simulated.
256 devices in a mesh: ep: 64 (over z, y, core), tp: 4 (over x).
Axes of the slice: x: 4, y: 4, z: 8, core: 2. Of those that a mesh axis runs over, the one named last changes fastest.
Arguments:
- tokens_a: bfloat16 [8192, 2048], P('ep'), may hold values from -30 to 30
- attn_gain: float32 [2048], replicated, may hold values from 0.1 to 1.9
- w_query: bfloat16 [2048, 2048], P(None, 'tp'), may hold values from -2 to 2
- w_query_rot: bfloat16 [2048, 1024], P(None, 'tp'), may hold values from -0.125 to 0.125
- w_latent: bfloat16 [2048, 512], replicated, may hold values from -2 to 2
- w_key_rot: bfloat16 [2048, 32], replicated, may hold values from -0.125 to 0.125
- latent_gain: float32 [512], replicated, may hold values from 0.1 to 1.9
- w_key_up: bfloat16 [512, 2048], P(None, 'tp'), may hold values from -2 to 2
- w_value_up: bfloat16 [512, 2048], P(None, 'tp'), may hold values from -0.25 to 0.25
- w_output: bfloat16 [2048, 2048], P('tp'), may hold values from -0.125 to 0.125
- tokens_b: bfloat16 [16384, 2048], P('ep'), may hold values from -6 to 6
- ffn_gain: float32 [2048], replicated, may hold values from 0.1 to 1.9
- expert_ids: int32 [16384, 2], P('ep'), may hold values from 0 to 63, all different within a row; in each aligned block of 256 rows (0 to 255, 256 to 511, ...) at most 16 rows name the same one
- expert_weights: float32 [16384, 2], P('ep'), may hold values from 0.1 to 1
- w_gate: bfloat16 [64, 2048, 1024], P('ep', None, 'tp'), may hold values from -0.125 to 0.125
- w_up: bfloat16 [64, 2048, 1024], P('ep', None, 'tp'), may hold values from -0.125 to 0.125
- w_down: bfloat16 [64, 1024, 2048], P('ep', 'tp'), may hold values from -0.1875 to 0.1875
Outputs:
- mixed_a: bfloat16 [8192, 2048], P(('ep', 'tp'))
- mixed_b: bfloat16 [16384, 2048], P('ep', 'tp')
Inputs may be any that keep to these rules, and one draw needn't show every extreme that they name: `expert_ids`: each row names 2 different experts. In the 256 rows of one index of ep no expert is named more than 16 times, and in some such block one expert is named exactly 16 times.
All inputs are finite; a program needn't handle non-finite values.
Results may differ from a plain program's by a relative error of at most 0.012.
Values may be sent and summed in bfloat16 or wider, within the bound.
No kernel may reach another device: no remote copies, remote signals or barrier semaphores. Data moves between devices by JAX's collectives and lax.ppermute only.
A program may use at most 192 MiB of HBM per device.

v0:
```python
import jax
import jax.numpy as jnp
from jax import lax
from jax.sharding import PartitionSpec as P

NOPE = 64
ROPE = 32
VD = 64
epsilon = 1e-06
rope_base = 10000.0


def normalize(matrix, gain):
    floats = matrix.astype(jnp.float32)
    scaled = floats * lax.rsqrt(jnp.mean(floats * floats, axis=-1, keepdims=True) + epsilon)
    return scaled * gain


def rotate(vectors, positions):
    rot_width = vectors.shape[-1]
    half_width = rot_width // 2
    inverse = rope_base ** (-(jnp.arange(half_width, dtype=jnp.float32) * 2.0) / rot_width)
    angles = positions.astype(jnp.float32)[:, None] * inverse[None, :]
    cosine = jnp.cos(angles)[:, None, :]
    sine_part = jnp.sin(angles)[:, None, :]
    first_half = vectors[..., :half_width]
    second_half = vectors[..., half_width:]
    return jnp.concatenate(
        [
            first_half * cosine - second_half * sine_part,
            first_half * sine_part + second_half * cosine,
        ],
        axis=-1,
    )


def attention_half(
    tokens_a,
    attn_gain,
    w_query,
    w_query_rot,
    w_latent,
    w_key_rot,
    latent_gain,
    w_key_up,
    w_value_up,
    w_output,
):
    row_count = tokens_a.shape[0]
    head_count = w_query.shape[1] // NOPE
    offset = lax.axis_index("ep") * row_count
    positions = offset + jnp.arange(row_count, dtype=jnp.int32)
    normed = normalize(tokens_a, attn_gain).astype(jnp.bfloat16)
    query_plain = jnp.dot(normed, w_query, preferred_element_type=jnp.float32).astype(jnp.bfloat16)
    query_plain = query_plain.reshape(row_count, head_count, NOPE)
    turned = jnp.dot(normed, w_query_rot, preferred_element_type=jnp.float32).reshape(
        row_count, head_count, ROPE
    )
    query_rotated_rows = rotate(turned, positions).astype(jnp.bfloat16)
    latent = normalize(
        jnp.dot(normed, w_latent, preferred_element_type=jnp.float32), latent_gain
    ).astype(jnp.bfloat16)
    key_raw = jnp.dot(normed, w_key_rot, preferred_element_type=jnp.float32)[:, None, :]
    key_turned = rotate(key_raw, positions)[:, 0, :].astype(jnp.bfloat16)
    logit_scale = (NOPE + ROPE) ** (-0.5)
    key_plain = jnp.dot(latent, w_key_up, preferred_element_type=jnp.float32).astype(jnp.bfloat16)
    values = jnp.dot(latent, w_value_up, preferred_element_type=jnp.float32).astype(jnp.bfloat16)
    update_key_plain = lax.all_gather(key_plain, "ep", axis=0, tiled=True)
    update_values = lax.all_gather(values, "ep", axis=0, tiled=True)
    key_count = update_key_plain.shape[0]
    blocks = key_count // row_count
    key_blocks = update_key_plain.reshape(blocks, row_count, head_count, NOPE)
    value_blocks = update_values.reshape(blocks, row_count, head_count, VD)
    rotated_key_blocks = lax.all_gather(key_turned, "ep", axis=0, tiled=True).reshape(
        blocks, row_count, ROPE
    )
    score_matrix = (
        jnp.einsum("yvz,wrvz->yvwr", query_plain, key_blocks, preferred_element_type=jnp.float32)
        + jnp.einsum(
            "yjx,inx->yjin",
            query_rotated_rows,
            rotated_key_blocks,
            preferred_element_type=jnp.float32,
        )
    ) * logit_scale
    key_pos = jnp.arange(key_count, dtype=jnp.int32).reshape(blocks, row_count)
    allowed = key_pos[None, None, :, :] <= positions[:, None, None, None]
    masked = jnp.where(allowed, score_matrix, -1e30)
    block_max = jnp.max(masked, axis=-1)
    probs = jnp.where(allowed, jnp.exp(masked - block_max[..., None]), 0.0)
    block_total = jnp.sum(probs, axis=-1)
    block_out = jnp.einsum(
        "qhbk,bkhd->qhbd",
        probs.astype(jnp.bfloat16),
        value_blocks,
        preferred_element_type=jnp.float32,
    )
    run_max = jnp.full((row_count, head_count), -1e30, jnp.float32)
    new_max = jnp.maximum(run_max, jnp.max(block_max, axis=-1))
    new_factor = jnp.exp(block_max - new_max[..., None])
    new_total = jnp.sum(new_factor * block_total, axis=-1)
    new_out = jnp.sum(new_factor[..., None] * block_out, axis=2)
    attended = (
        (new_out / new_total[..., None]).astype(jnp.bfloat16).reshape(row_count, head_count * VD)
    )
    return lax.psum_scatter(
        jnp.dot(attended, w_output, preferred_element_type=jnp.float32).astype(jnp.bfloat16),
        "tp",
        scatter_dimension=0,
        tiled=True,
    )


def expert_half(tokens_b, ffn_gain, expert_ids, expert_weights, w_gate, w_up, w_down):
    row_count = tokens_b.shape[0]
    top_count = expert_ids.shape[1]
    expert_count = w_gate.shape[0] * lax.axis_size("ep")
    capacity = 2 * row_count * top_count // expert_count
    normed = normalize(tokens_b, ffn_gain).astype(jnp.bfloat16)
    flat_ids = expert_ids.reshape(-1)
    pair_count = flat_ids.shape[0]
    onehot = (flat_ids[:, None] == jnp.arange(expert_count, dtype=jnp.int32)[None, :]).astype(
        jnp.int32
    )
    before = jnp.cumsum(onehot, axis=0) - onehot
    slot_index = jnp.sum(before * onehot, axis=1)
    target = flat_ids * capacity + slot_index
    source_row = (
        jnp.zeros((expert_count * capacity,), jnp.int32)
        .at[target]
        .set(jnp.arange(pair_count, dtype=jnp.int32) // top_count)
    )
    occupied = jnp.zeros((expert_count * capacity,), jnp.int32).at[target].set(1)
    outgoing = jnp.where(occupied[:, None] > 0, normed[source_row], jnp.zeros((), jnp.bfloat16))
    outgoing = outgoing.reshape(expert_count, capacity, normed.shape[1])
    gate_weight = w_gate[0]
    up_weight = w_up[0]
    down_weight = w_down[0]
    arrived = lax.all_to_all(outgoing, "ep", split_axis=0, concat_axis=0, tiled=True)
    flat_rows = arrived.reshape(-1, arrived.shape[-1])
    gate_part = jnp.dot(flat_rows, gate_weight, preferred_element_type=jnp.float32)
    up_part = jnp.dot(flat_rows, up_weight, preferred_element_type=jnp.float32)
    hidden_rows = (jax.nn.silu(gate_part) * up_part).astype(jnp.bfloat16)
    hidden = hidden_rows.reshape(arrived.shape[0], arrived.shape[1], gate_weight.shape[1])
    partial_value = jnp.dot(
        hidden.reshape(-1, hidden.shape[-1]), down_weight, preferred_element_type=jnp.float32
    )
    partial_value = partial_value.reshape(expert_count, capacity, down_weight.shape[1])
    summed = lax.psum_scatter(
        partial_value.astype(jnp.bfloat16), "tp", scatter_dimension=2, tiled=True
    )
    returned = lax.all_to_all(summed, "ep", split_axis=0, concat_axis=0, tiled=True)
    picked = returned.reshape(expert_count * capacity, -1)[target].astype(jnp.float32)
    picked = picked.reshape(row_count, top_count, -1)
    shares = expert_weights / jnp.sum(expert_weights, axis=1, keepdims=True)
    return jnp.sum(picked * shares[:, :, None], axis=1).astype(jnp.bfloat16)


def on_device(
    tokens_a,
    attn_gain,
    w_query,
    w_query_rot,
    w_latent,
    w_key_rot,
    latent_gain,
    w_key_up,
    w_value_up,
    w_output,
    tokens_b,
    ffn_gain,
    expert_ids,
    expert_weights,
    w_gate,
    w_up,
    w_down,
):
    mixed_a = attention_half(
        tokens_a,
        attn_gain,
        w_query,
        w_query_rot,
        w_latent,
        w_key_rot,
        latent_gain,
        w_key_up,
        w_value_up,
        w_output,
    )
    mixed_b = expert_half(tokens_b, ffn_gain, expert_ids, expert_weights, w_gate, w_up, w_down)
    return (mixed_a, mixed_b)


def solution(mesh):
    placed = (
        P("ep", None),
        P(),
        P(None, "tp"),
        P(None, "tp"),
        P(),
        P(),
        P(),
        P(None, "tp"),
        P(None, "tp"),
        P("tp", None),
        P("ep", None),
        P(),
        P("ep", None),
        P("ep", None),
        P("ep", None, "tp"),
        P("ep", None, "tp"),
        P("ep", "tp", None),
    )
    return jax.shard_map(
        on_device,
        mesh=mesh,
        in_specs=placed,
        out_specs=(P(("ep", "tp"), None), P("ep", "tp")),
        check_vma=False,
    )
```

profile of v0, /device:TPU:8, one launch (start us, length us, event | category | flops | bytes accessed | tf_op | source)
XLA Modules:
  0.0 389.7 jit_solution(2353448182346201327)
XLA Ops:
  8.1 1.4 fusion.23
  9.4 2.4 multiply_reduce_fusion.2
  11.8 2.0 convolution_convert_fusion.4
  13.9 2.0 convolution_convert_fusion.2
  17.0 1.2 reduce-window.6
  19.6 2.4 scatter_custom_fusion.1
  22.1 2.4 scatter_custom_fusion
  24.6 1.5 fusion.19
  26.2 1.5 fusion.21
  27.7 6.0 %gather_fusion = bf16[1024,2048]{1,0:T(8,128)(2,1)} fusion(bf16[256,2048]{1,0:T(8,128)(2,1)S(1)} %fusion.21, s32[1024]{0:T(1024)S(1)} %fusion.47), kind=kCustom, calls=%fused_computation | custom fusion | bytes 8392704 | tf_op jit(solution)/shard_map/gather | solution.py:134
  33.7 4.6 %broadcast_select_fusion = bf16[64,16,2048]{2,1,0:T(8,128)(2,1)} fusion(bf16[64,16,2048]{2,1,0:T(8,128)(2,1)} %bitcast.79, pred[64,16]{1,0:T(8,128)(4,1)S(1)} %broadcast_in_dim.76), kind=kLoop, calls=%fused_computation.19 | loop fusion | flops 2097152 | bytes 8389632 | tf_op jit(solution)/shard_map/jit(_where)/select_n | solution.py:134
  38.3 12.3 %all-to-all-start = ((bf16[64,16,2048]{2,1,0:T(8,128)(2,1)}), bf16[64,16,2048]{2,1,0:T(8,128)(2,1)}, u32[]{:S(2)}, u32[]{:S(2)}) async-start(bf16[64,16,2048]{2,1,0:T(8,128)(2,1)} %broadcast_select_fusion), calls=%async_computation.1 | async-start | bytes 8388608 | tf_op jit(solution)/shard_map/all_to_all | solution.py:139
  51.2 154.9 %all-gather = bf16[8192,1,32]{0,2,1:T(8,128)(2,1)S(1)} all-gather(bf16[128,1,32]{0,2,1:T(8,128)(2,1)S(1)} %pad_maximum_fusion), channel_id=2, replica_groups=mesh['ep'=64,'tp'=4] {'ep'}, dimensions={0}, use_global_device_ids=true | all-gather | bytes 532480 | tf_op jit(solution)/shard_map/all_gather | solution.py:74
  206.1 1.8 fusion.59
  208.0 2.1 convolution_convert_fusion.3
  210.1 4.2 %fusion.28 = f32[1024,256]{1,0:T(8,128)S(1)} fusion(bf16[1024,2048]{1,0:T(8,128)(2,1)} %bitcast.15, bf16[1,2048,256]{2,1,0:T(8,128)(2,1)} %param.31), kind=kOutput, calls=%fused_computation.41 | convolution fusion | flops 1073741824 | bytes 6291456 | tf_op jit(solution)/shard_map/dot_general | solution.py:141
  214.4 3.9 fusion.22
  218.3 3.2 convolution_convert_fusion
  222.6 1.6 broadcast_compare_fusion
  224.2 14.9 %fusion.30 = f32[128,8,64,128]{0,3,2,1:T(8,128)} fusion(bf16[64,128,32]{1,0,2:T(8,128)(2,1)} %bitcast.80, bf16[128,8,16]{0,2,1:T(8,128)(2,1)S(1)} %get-tuple-element.7, bf16[128,8,16]{0,2,1:T(8,128)(2,1)S(1)} %get-tuple-element.6), kind=kOutput, calls=%fused_computation.44 | convolution fusion | flops 537001984 | bytes 34144256 | tf_op jit(solution)/shard_map/yjx,inx->yjin/dot_general | solution.py:79
  239.1 21.2 %reshape.303 = bf16[64,128,8,64]{3,2,1,0:T(8,128)(2,1)} reshape(bf16[8192,512]{1,0:T(8,128)(2,1)} %all-gather.4.cloned.1.call-done) | data formatting | bytes 16777216 | tf_op jit(solution)/shard_map/reshape | solution.py:72
  260.4 21.2 %reshape.304 = bf16[64,128,8,64]{3,2,1,0:T(8,128)(2,1)} reshape(bf16[8192,512]{1,0:T(8,128)(2,1)} %all-gather.6.cloned.1.call-done) | data formatting | bytes 16777216 | tf_op jit(solution)/shard_map/reshape | solution.py:73
  281.6 27.4 %fusion.64 = (f32[128,8,64]{0,2,1:T(8,128)S(1)}, f32[128,8,64,128]{0,3,2,1:T(8,128)}) fusion(f32[128,8,64,128]{0,3,2,1:T(8,128)} %fusion.30, bf16[128,8,64,1]{0,2,3,1:T(8,128)(2,1)S(1)} %bitcast.82, bf16[64,128,8,64]{3,2,1,0:T(8,128)(2,1)} %reshape.303, pred[128,64,128]{0,2,1:T(8,128)(4,1)S(1)} %broadcast_compare_fusion), kind=kOutput, calls=%fused_computation.109 | convolution fusion | flops 1107230720 | bytes 76939264 | tf_op jit(solution)/shard_map/yvz,wrvz->yvwr/dot_general | solution.py:78
  309.0 16.1 %fusion.2 = (f32[128,8,64]{0,2,1:T(8,128)S(1)}, f32[128,8]{0,1:T(8,128)S(1)}) fusion(f32[128,8,64,128]{0,3,2,1:T(8,128)} %get-tuple-element.15, f32[128,8,64]{0,2,1:T(8,128)S(1)} %get-tuple-element.14, pred[128,64,128]{0,2,1:T(8,128)(4,1)S(1)} %broadcast_compare_fusion), kind=kLoop, calls=%fused_computation.8 | loop fusion | flops 33487872 | bytes 35131392 | tf_op jit(solution)/shard_map/reduce_sum | solution.py:91
  325.9 8.3 %all-to-all-start.1 = ((bf16[64,16,512]{2,1,0:T(8,128)(2,1)}), bf16[64,16,512]{2,1,0:T(8,128)(2,1)}, u32[]{:S(2)}, u32[]{:S(2)}) async-start(bf16[64,16,512]{2,1,0:T(8,128)(2,1)} %reduce-scatter.5.cloned.1.call-done), calls=%async_computation.3 | async-start | bytes 2097152 | tf_op jit(solution)/shard_map/all_to_all | solution.py:152
  334.2 20.3 %fusion.6 = f32[128,8,64]{0,2,1:T(8,128)} fusion(f32[128,8,64]{0,2,1:T(8,128)} %get-tuple-element.5, f32[128,8,64,128]{0,3,2,1:T(8,128)} %get-tuple-element.15, f32[128,8,64]{0,2,1:T(8,128)S(1)} %get-tuple-element.14, pred[128,64,128]{0,2,1:T(8,128)(4,1)S(1)} %broadcast_compare_fusion, bf16[64,128,8,64]{3,2,1,0:T(8,128)(2,1)} %reshape.304), kind=kOutput, calls=%fused_computation.12 | convolution fusion | flops 1107230720 | bytes 43778048 | tf_op jit(solution)/shard_map/qhbk,bkhd->qhbd/dot_general | solution.py:92
  355.5 1.3 convolution_convert_fusion.1
  357.0 5.8 %all-to-all-done.1 = bf16[64,16,512]{2,1,0:T(8,128)(2,1)} async-done(((bf16[64,16,512]{2,1,0:T(8,128)(2,1)}), bf16[64,16,512]{2,1,0:T(8,128)(2,1)}, u32[]{:S(2)}, u32[]{:S(2)}) %all-to-all-start.1) | async-done | bytes 1048608 | tf_op jit(solution)/shard_map/all_to_all | solution.py:152
  362.9 4.0 %gather_fusion.1 = bf16[512,512]{1,0:T(8,128)(2,1)} fusion(bf16[1024,512]{1,0:T(8,128)(2,1)} %bitcast.21, s32[1024]{0:T(1024)S(1)} %pad_clamp_fusion), kind=kCustom, calls=%fused_computation.1 | custom fusion | bytes 1050624 | tf_op jit(solution)/shard_map/gather | solution.py:153
  366.9 1.7 reshape.263
  368.6 2.1 multiply_reduce_fusion
  370.6 11.7 %reduce-scatter.3.cloned.1.call-done = bf16[32,2048]{1,0:T(8,128)(2,1)} async-done(((bf16[128,2048]{1,0:T(8,128)(2,1)}), bf16[32,2048]{1,0:T(8,128)(2,1)}) %reduce-scatter.3.cloned.1.call-update) | async-done | bytes 131088 | tf_op jit(solution)/shard_map/reduce_scatter | solution.py:106
  (62 shorter events, 6.5 us)
Async XLA Ops:
  8.0 347.5 %copy-start = (bf16[512,2048]{1,0:T(8,128)(2,1)S(1)}, bf16[512,2048]{1,0:T(8,128)(2,1)}, u32[]{:S(2)}) copy-start(bf16[512,2048]{1,0:T(8,128)(2,1)} %param.26) | copy-start | bytes 6291460
  8.0 231.1 %all-gather.4.cloned.1.call-start = ((), (), s32[]{:S(2)}) async-start(), calls=%async_computation.4 | async-start | bytes 8519680 | tf_op jit(solution)/shard_map/all_gather | solution.py:68
  13.8 246.5 %all-gather.6.cloned.1.call-start = ((), (), s32[]{:S(2)}) async-start(), calls=%async_computation.5 | async-start | bytes 8519680 | tf_op jit(solution)/shard_map/all_gather | solution.py:69
  33.7 16.9 %copy-start.2 = (bf16[128,2048]{1,0:T(8,128)(2,1)S(1)}, bf16[128,2048]{1,0:T(8,128)(2,1)}, u32[]{:S(2)}) copy-start(bf16[128,2048]{1,0:T(8,128)(2,1)} %param.17) | copy-start | bytes 1572868
  33.7 16.9 %copy-start.4 = (bf16[2048,32]{0,1:T(8,128)(2,1)S(1)}, bf16[2048,32]{0,1:T(8,128)(2,1)}, u32[]{:S(2)}) copy-start(bf16[2048,32]{0,1:T(8,128)(2,1)} %param.22) | copy-start | bytes 393220
  33.7 17.0 %copy-start.5 = (f32[2048]{0:T(1024)S(1)}, f32[2048]{0:T(1024)}, u32[]{:S(2)}) copy-start(f32[2048]{0:T(1024)} %param.18) | copy-start | bytes 24580
  38.3 171.8 %all-to-all-start = ((bf16[64,16,2048]{2,1,0:T(8,128)(2,1)}), bf16[64,16,2048]{2,1,0:T(8,128)(2,1)}, u32[]{:S(2)}, u32[]{:S(2)}) async-start(bf16[64,16,2048]{2,1,0:T(8,128)(2,1)} %broadcast_select_fusion), calls=%async_computation.1 | async-start | bytes 8388608 | tf_op jit(solution)/shard_map/all_to_all | solution.py:139
  50.6 275.3 %reduce-scatter.5.cloned.1.call-start = ((), (), s32[]{:S(2)}) async-start(), calls=%async_computation.7 | async-start | bytes 5242880 | tf_op jit(solution)/shard_map/reduce_scatter | solution.py:149
  210.1 8.1 %copy-start.1 = (bf16[1,256,2048]{2,1,0:T(8,128)(2,1)S(1)}, bf16[1,256,2048]{2,1,0:T(8,128)(2,1)}, u32[]{:S(2)}) copy-start(bf16[1,256,2048]{2,1,0:T(8,128)(2,1)} %param.33) | copy-start | bytes 3145732
  325.9 37.0 %all-to-all-start.1 = ((bf16[64,16,512]{2,1,0:T(8,128)(2,1)}), bf16[64,16,512]{2,1,0:T(8,128)(2,1)}, u32[]{:S(2)}, u32[]{:S(2)}) async-start(bf16[64,16,512]{2,1,0:T(8,128)(2,1)} %reduce-scatter.5.cloned.1.call-done), calls=%async_computation.3 | async-start | bytes 2097152 | tf_op jit(solution)/shard_map/all_to_all | solution.py:152
  334.2 48.1 %reduce-scatter.3.cloned.1.call-start = ((), (), s32[]{:S(2)}) async-start(), calls=%async_computation.6 | async-start | bytes 655360 | tf_op jit(solution)/shard_map/reduce_scatter | solution.py:106
  334.2 22.6 %copy-start.3 = (f32[256,2]{0,1:T(2,128)S(1)}, f32[256,2]{0,1:T(2,128)}, u32[]{:S(2)}) copy-start(f32[256,2]{0,1:T(2,128)} %param.30) | copy-start | bytes 6148
Sparse Core Ops, SparseCore 0:
  13.9 129.2 all-gather.3
  146.6 82.3 all-gather.5
Sparse Core Ops, SparseCore 1:
  221.6 48.2 reduce-scatter.4
  356.9 25.3 reduce-scatter.2
where the time goes:
time: 392 us; the launch traced here: 390 us
  blocking collectives  155 us (40%)
  matrix products  85.8 us (22%)
  local copies, waits for them, and re-layouts  61.9 us (16%)
  other arithmetic  33 us (8%)
  starting transfers between devices  20.7 us (5%)
  waiting for transfers between devices  17.6 us (4%)
  between operations  15.8 us (4%)
    all_gather x1, blocking collectives, attention_half(): lax.all_gather(key_turned, 'ep', axis=0, tiled=True)  155 us
    dot_general x1, matrix products, attention_half(): jnp.einsum('yvz,wrvz->yvwr', query_plain, key_blocks, preferred_element_t...  27.4 us
    reshape x1, local copies, waits for them, and re-layouts, attention_half(): key_blocks = update_key_plain.reshape(blocks, row_count, head_count, NOPE)  21.2 us
    reshape x1, local copies, waits for them, and re-layouts, attention_half(): value_blocks = update_values.reshape(blocks, row_count, head_count, VD)  21.2 us
    dot_general x1, matrix products, attention_half(): jnp.einsum('qhbk,bkhd->qhbd', probs.astype(jnp.bfloat16), value_blocks, p...  20.3 us
    reduce_sum x1, other arithmetic, attention_half(): block_total = jnp.sum(probs, axis=-1)  16.1 us
    dot_general x1, matrix products, attention_half(): jnp.einsum('yjx,inx->yjin', query_rotated_rows, rotated_key_blocks, prefe...  14.9 us
    all_to_all x1, starting transfers between devices, expert_half(): lax.all_to_all(outgoing, 'ep', split_axis=0, concat_axis=0, tiled=True)  12.3 us
  transfers between devices with their start and end apart: 6, of which 2 were waited for; matrix products, arithmetic and copies ran while one was open for 45% of the time, Pallas kernels for 0%

commit v1 on v0

--- a/solution.py
+++ b/solution.py
@@ -8,6 +8,14 @@
 VD = 64
 epsilon = 1e-06
 rope_base = 10000.0
+
+
+def tiled_gather(value, axis, dim):
+    count = lax.axis_size(axis)
+    repeats = [count if d == dim else 1 for d in range(value.ndim)]
+    return lax.all_to_all(
+        jnp.tile(value, repeats), axis, split_axis=dim, concat_axis=dim, tiled=True
+    )
 
 
 def normalize(matrix, gain):
@@ -71,9 +79,7 @@
     blocks = key_count // row_count
     key_blocks = update_key_plain.reshape(blocks, row_count, head_count, NOPE)
     value_blocks = update_values.reshape(blocks, row_count, head_count, VD)
-    rotated_key_blocks = lax.all_gather(key_turned, "ep", axis=0, tiled=True).reshape(
-        blocks, row_count, ROPE
-    )
+    rotated_key_blocks = tiled_gather(key_turned, "ep", 0).reshape(blocks, row_count, ROPE)
     score_matrix = (
         jnp.einsum("yvz,wrvz->yvwr", query_plain, key_blocks, preferred_element_type=jnp.float32)
         + jnp.einsum(

time: 392 us -> 361 us (0.921)
  blocking collectives: 155 us -> 0 us
  waiting for transfers between devices: 17.6 us -> 135 us
  starting transfers between devices: 20.7 us -> 27 us
    all_gather x1 -> x0, blocking collectives: 155 us -> none  [attention_half(): lax.all_gather(key_turned, 'ep', axis=0, tiled=True)]
    all_to_all x1, waiting for transfers between devices: 0.01 us -> 110 us  [expert_half(): lax.all_to_all(outgoing, 'ep', split_axis=0, concat_axis=0, tiled=True)]
    all_to_all x0 -> x1, starting transfers between devices: none -> 6.84 us  [tiled_gather(): lax.all_to_all(jnp.tile(value, repeats), axis, split_axis=dim, concat_axi...]
    all_to_all x0 -> x1, waiting for transfers between devices: none -> 6.57 us  [tiled_gather(): lax.all_to_all(jnp.tile(value, repeats), axis, split_axis=dim, concat_axi...]
  transfers between devices with their start and end apart: 6 -> 7, of which waited for: 2 -> 5; matrix products, arithmetic and copies ran while one was open for 45% -> 49% of each run, Pallas kernels for 0% -> 0%
where the time goes in v1:
time: 361 us; the launch traced here: 359 us
  waiting for transfers between devices  135 us (37%)
  matrix products  85.8 us (24%)
  local copies, waits for them, and re-layouts  62.1 us (17%)
  other arithmetic  32.8 us (9%)
  starting transfers between devices  27 us (7%)
  between operations  15.8 us (4%)
    all_to_all x1, waiting for transfers between devices, expert_half(): lax.all_to_all(outgoing, 'ep', split_axis=0, concat_axis=0, tiled=True)  110 us
    dot_general x1, matrix products, attention_half(): jnp.einsum('yvz,wrvz->yvwr', query_plain, key_blocks, preferred_element_t...  27.4 us
    reshape x1, local copies, waits for them, and re-layouts, attention_half(): key_blocks = update_key_plain.reshape(blocks, row_count, head_count, NOPE)  21.5 us
    reshape x1, local copies, waits for them, and re-layouts, attention_half(): value_blocks = update_values.reshape(blocks, row_count, head_count, VD)  21.2 us
    dot_general x1, matrix products, attention_half(): jnp.einsum('qhbk,bkhd->qhbd', probs.astype(jnp.bfloat16), value_blocks, p...  20 us
    reduce_sum x1, other arithmetic, attention_half(): block_total = jnp.sum(probs, axis=-1)  16.1 us
    dot_general x1, matrix products, attention_half(): jnp.einsum('yjx,inx->yjin', query_rotated_rows, rotated_key_blocks, prefe...  16.1 us
    all_to_all x1, starting transfers between devices, expert_half(): lax.all_to_all(outgoing, 'ep', split_axis=0, concat_axis=0, tiled=True)  12.3 us
  transfers between devices with their start and end apart: 7, of which 5 were waited for; matrix products, arithmetic and copies ran while one was open for 49% of the time, Pallas kernels for 0%

profile of v1, /device:TPU:8, one launch (start us, length us, event | category | flops | bytes accessed | tf_op | source)
XLA Modules:
  0.0 358.7 jit_solution(8720664844643153763)
XLA Ops:
  8.1 1.4 fusion.23
  9.4 2.4 multiply_reduce_fusion.2
  11.8 2.0 convolution_convert_fusion.4
  13.9 2.0 convolution_convert_fusion.2
  19.6 2.4 scatter_custom_fusion.1
  22.1 2.4 scatter_custom_fusion
  24.6 1.5 fusion.19
  26.2 1.5 fusion.21
  27.7 6.0 %gather_fusion = bf16[1024,2048]{1,0:T(8,128)(2,1)} fusion(bf16[256,2048]{1,0:T(8,128)(2,1)S(1)} %fusion.21, s32[1024]{0:T(1024)S(1)} %fusion.46), kind=kCustom, calls=%fused_computation | custom fusion | bytes 8392704 | tf_op jit(solution)/shard_map/gather | solution.py:140
  33.7 4.6 %broadcast_select_fusion = bf16[64,16,2048]{2,1,0:T(8,128)(2,1)} fusion(bf16[64,16,2048]{2,1,0:T(8,128)(2,1)} %bitcast.76, pred[64,16]{1,0:T(8,128)(4,1)S(1)} %broadcast_in_dim.76), kind=kLoop, calls=%fused_computation.19 | loop fusion | flops 2097152 | bytes 8389632 | tf_op jit(solution)/shard_map/jit(_where)/select_n | solution.py:140
  38.3 12.3 %all-to-all-start.1 = ((bf16[64,16,2048]{2,1,0:T(8,128)(2,1)}), bf16[64,16,2048]{2,1,0:T(8,128)(2,1)}, u32[]{:S(2)}, u32[]{:S(2)}) async-start(bf16[64,16,2048]{2,1,0:T(8,128)(2,1)} %broadcast_select_fusion), calls=%async_computation.2 | async-start | bytes 8388608 | tf_op jit(solution)/shard_map/all_to_all | solution.py:145
  51.3 1.8 fusion.58
  53.1 2.1 convolution_convert_fusion.3
  55.2 110.3 %all-to-all-done.1 = bf16[64,16,2048]{2,1,0:T(8,128)(2,1)} async-done(((bf16[64,16,2048]{2,1,0:T(8,128)(2,1)}), bf16[64,16,2048]{2,1,0:T(8,128)(2,1)}, u32[]{:S(2)}, u32[]{:S(2)}) %all-to-all-start.1) | async-done | bytes 4194336 | tf_op jit(solution)/shard_map/all_to_all | solution.py:145
  166.4 6.8 %all-to-all-start = ((bf16[64,128,32]{1,2,0:T(8,128)(2,1)}), bf16[64,128,32]{1,2,0:T(8,128)(2,1)}, u32[]{:S(2)}, u32[]{:S(2)}) async-start(bf16[64,128,32]{1,2,0:T(8,128)(2,1)} %tile.2), calls=%async_computation | async-start | bytes 1048576 | tf_op jit(solution)/shard_map/all_to_all | solution.py:16
  173.5 3.8 %fusion.28 = f32[1024,256]{1,0:T(8,128)S(1)} fusion(bf16[1024,2048]{1,0:T(8,128)(2,1)} %bitcast.16, bf16[1,2048,256]{2,1,0:T(8,128)(2,1)} %param.31), kind=kOutput, calls=%fused_computation.41 | convolution fusion | flops 1073741824 | bytes 6291456 | tf_op jit(solution)/shard_map/dot_general | solution.py:147
  177.3 3.5 fusion.22
  180.8 3.2 convolution_convert_fusion
  184.2 1.4 broadcast_compare_fusion
  185.6 6.6 %all-to-all-done = bf16[64,128,32]{1,2,0:T(8,128)(2,1)} async-done(((bf16[64,128,32]{1,2,0:T(8,128)(2,1)}), bf16[64,128,32]{1,2,0:T(8,128)(2,1)}, u32[]{:S(2)}, u32[]{:S(2)}) %all-to-all-start) | async-done | bytes 524320 | tf_op jit(solution)/shard_map/all_to_all | solution.py:16
  192.2 16.1 %fusion.30 = f32[128,8,64,128]{0,3,2,1:T(8,128)} fusion(bf16[64,128,32]{1,2,0:T(8,128)(2,1)} %all-to-all-done, bf16[128,8,16]{0,2,1:T(8,128)(2,1)S(1)} %get-tuple-element.7, bf16[128,8,16]{0,2,1:T(8,128)(2,1)S(1)} %get-tuple-element.6), kind=kOutput, calls=%fused_computation.44 | convolution fusion | flops 537001984 | bytes 34144256 | tf_op jit(solution)/shard_map/yjx,inx->yjin/dot_general | solution.py:85
  208.2 21.5 %reshape.310 = bf16[64,128,8,64]{3,2,1,0:T(8,128)(2,1)} reshape(bf16[8192,512]{1,0:T(8,128)(2,1)} %all-gather.3.cloned.1.call-done) | data formatting | bytes 16777216 | tf_op jit(solution)/shard_map/reshape | solution.py:80
  230.6 21.2 %reshape.311 = bf16[64,128,8,64]{3,2,1,0:T(8,128)(2,1)} reshape(bf16[8192,512]{1,0:T(8,128)(2,1)} %all-gather.5.cloned.1.call-done) | data formatting | bytes 16777216 | tf_op jit(solution)/shard_map/reshape | solution.py:81
  251.8 27.4 %fusion.63 = (f32[128,8,64]{0,2,1:T(8,128)S(1)}, f32[128,8,64,128]{0,3,2,1:T(8,128)}) fusion(f32[128,8,64,128]{0,3,2,1:T(8,128)} %fusion.30, bf16[128,8,64,1]{0,2,3,1:T(8,128)(2,1)S(1)} %bitcast.77, bf16[64,128,8,64]{3,2,1,0:T(8,128)(2,1)} %reshape.310, pred[128,64,128]{0,2,1:T(8,128)(4,1)S(1)} %broadcast_compare_fusion), kind=kOutput, calls=%fused_computation.108 | convolution fusion | flops 1107230720 | bytes 76939264 | tf_op jit(solution)/shard_map/yvz,wrvz->yvwr/dot_general | solution.py:84
  279.3 16.1 %fusion.2 = (f32[128,8,64]{0,2,1:T(8,128)S(1)}, f32[128,8]{0,1:T(8,128)S(1)}) fusion(f32[128,8,64,128]{0,3,2,1:T(8,128)} %get-tuple-element.15, f32[128,8,64]{0,2,1:T(8,128)S(1)} %get-tuple-element.14, pred[128,64,128]{0,2,1:T(8,128)(4,1)S(1)} %broadcast_compare_fusion), kind=kLoop, calls=%fused_computation.8 | loop fusion | flops 33487872 | bytes 35131392 | tf_op jit(solution)/shard_map/reduce_sum | solution.py:97
  296.2 7.5 %all-to-all-start.2 = ((bf16[64,16,512]{2,1,0:T(8,128)(2,1)}), bf16[64,16,512]{2,1,0:T(8,128)(2,1)}, u32[]{:S(2)}, u32[]{:S(2)}) async-start(bf16[64,16,512]{2,1,0:T(8,128)(2,1)} %reduce-scatter.5.cloned.1.call-done), calls=%async_computation.4 | async-start | bytes 2097152 | tf_op jit(solution)/shard_map/all_to_all | solution.py:158
  303.7 20.0 %fusion.6 = f32[128,8,64]{0,2,1:T(8,128)} fusion(f32[128,8,64]{0,2,1:T(8,128)} %get-tuple-element.5, f32[128,8,64,128]{0,3,2,1:T(8,128)} %get-tuple-element.15, f32[128,8,64]{0,2,1:T(8,128)S(1)} %get-tuple-element.14, pred[128,64,128]{0,2,1:T(8,128)(4,1)S(1)} %broadcast_compare_fusion, bf16[64,128,8,64]{3,2,1,0:T(8,128)(2,1)} %reshape.311), kind=kOutput, calls=%fused_computation.12 | convolution fusion | flops 1107230720 | bytes 43778048 | tf_op jit(solution)/shard_map/qhbk,bkhd->qhbd/dot_general | solution.py:98
  326.2 6.1 %all-to-all-done.2 = bf16[64,16,512]{2,1,0:T(8,128)(2,1)} async-done(((bf16[64,16,512]{2,1,0:T(8,128)(2,1)}), bf16[64,16,512]{2,1,0:T(8,128)(2,1)}, u32[]{:S(2)}, u32[]{:S(2)}) %all-to-all-start.2) | async-done | bytes 1048608 | tf_op jit(solution)/shard_map/all_to_all | solution.py:158
  332.3 4.0 %gather_fusion.1 = bf16[512,512]{1,0:T(8,128)(2,1)} fusion(bf16[1024,512]{1,0:T(8,128)(2,1)} %bitcast.22, s32[1024]{0:T(1024)S(1)} %pad_clamp_fusion), kind=kCustom, calls=%fused_computation.1 | custom fusion | bytes 1050624 | tf_op jit(solution)/shard_map/gather | solution.py:159
  336.4 1.7 reshape.272
  338.0 2.1 multiply_reduce_fusion
  340.1 11.2 %reduce-scatter.3.cloned.1.call-done = bf16[32,2048]{1,0:T(8,128)(2,1)} async-done(((bf16[128,2048]{1,0:T(8,128)(2,1)}), bf16[32,2048]{1,0:T(8,128)(2,1)}) %reduce-scatter.3.cloned.1.call-update) | async-done | bytes 131088 | tf_op jit(solution)/shard_map/reduce_scatter | solution.py:112
  (65 shorter events, 10.0 us)
Async XLA Ops:
  8.0 316.8 %copy-start = (bf16[512,2048]{1,0:T(8,128)(2,1)S(1)}, bf16[512,2048]{1,0:T(8,128)(2,1)}, u32[]{:S(2)}) copy-start(bf16[512,2048]{1,0:T(8,128)(2,1)} %param.26) | copy-start | bytes 6291460
  8.0 200.2 %all-gather.3.cloned.1.call-start = ((), (), s32[]{:S(2)}) async-start(), calls=%async_computation.5 | async-start | bytes 8519680 | tf_op jit(solution)/shard_map/all_gather | solution.py:76
  13.8 216.8 %all-gather.5.cloned.1.call-start = ((), (), s32[]{:S(2)}) async-start(), calls=%async_computation.6 | async-start | bytes 8519680 | tf_op jit(solution)/shard_map/all_gather | solution.py:77
  33.7 16.9 %copy-start.2 = (bf16[128,2048]{1,0:T(8,128)(2,1)S(1)}, bf16[128,2048]{1,0:T(8,128)(2,1)}, u32[]{:S(2)}) copy-start(bf16[128,2048]{1,0:T(8,128)(2,1)} %param.17) | copy-start | bytes 1572868
  33.7 16.9 %copy-start.5 = (bf16[2048,32]{0,1:T(8,128)(2,1)S(1)}, bf16[2048,32]{0,1:T(8,128)(2,1)}, u32[]{:S(2)}) copy-start(bf16[2048,32]{0,1:T(8,128)(2,1)} %param.22) | copy-start | bytes 393220
  33.7 16.9 %copy-start.6 = (f32[2048]{0:T(1024)S(1)}, f32[2048]{0:T(1024)}, u32[]{:S(2)}) copy-start(f32[2048]{0:T(1024)} %param.18) | copy-start | bytes 24580
  38.3 127.2 %all-to-all-start.1 = ((bf16[64,16,2048]{2,1,0:T(8,128)(2,1)}), bf16[64,16,2048]{2,1,0:T(8,128)(2,1)}, u32[]{:S(2)}, u32[]{:S(2)}) async-start(bf16[64,16,2048]{2,1,0:T(8,128)(2,1)} %broadcast_select_fusion), calls=%async_computation.2 | async-start | bytes 8388608 | tf_op jit(solution)/shard_map/all_to_all | solution.py:145
  166.4 10.9 %copy-start.4 = (bf16[1,2048,256]{2,1,0:T(8,128)(2,1)S(1)}, bf16[1,2048,256]{2,1,0:T(8,128)(2,1)}, u32[]{:S(2)}) copy-start(bf16[1,2048,256]{2,1,0:T(8,128)(2,1)} %param.32) | copy-start | bytes 3145732
  166.4 25.8 %all-to-all-start = ((bf16[64,128,32]{1,2,0:T(8,128)(2,1)}), bf16[64,128,32]{1,2,0:T(8,128)(2,1)}, u32[]{:S(2)}, u32[]{:S(2)}) async-start(bf16[64,128,32]{1,2,0:T(8,128)(2,1)} %tile.2), calls=%async_computation | async-start | bytes 1048576 | tf_op jit(solution)/shard_map/all_to_all | solution.py:16
  173.2 122.9 %reduce-scatter.5.cloned.1.call-start = ((), (), s32[]{:S(2)}) async-start(), calls=%async_computation.8 | async-start | bytes 5242880 | tf_op jit(solution)/shard_map/reduce_scatter | solution.py:155
  173.5 7.3 %copy-start.1 = (bf16[1,256,2048]{2,1,0:T(8,128)(2,1)S(1)}, bf16[1,256,2048]{2,1,0:T(8,128)(2,1)}, u32[]{:S(2)}) copy-start(bf16[1,256,2048]{2,1,0:T(8,128)(2,1)} %param.33) | copy-start | bytes 3145732
  296.2 36.2 %all-to-all-start.2 = ((bf16[64,16,512]{2,1,0:T(8,128)(2,1)}), bf16[64,16,512]{2,1,0:T(8,128)(2,1)}, u32[]{:S(2)}, u32[]{:S(2)}) async-start(bf16[64,16,512]{2,1,0:T(8,128)(2,1)} %reduce-scatter.5.cloned.1.call-done), calls=%async_computation.4 | async-start | bytes 2097152 | tf_op jit(solution)/shard_map/all_to_all | solution.py:158
  303.7 47.6 %reduce-scatter.3.cloned.1.call-start = ((), (), s32[]{:S(2)}) async-start(), calls=%async_computation.7 | async-start | bytes 655360 | tf_op jit(solution)/shard_map/reduce_scatter | solution.py:112
  303.7 22.3 %copy-start.3 = (f32[256,2]{0,1:T(2,128)S(1)}, f32[256,2]{0,1:T(2,128)}, u32[]{:S(2)}) copy-start(f32[256,2]{0,1:T(2,128)} %param.30) | copy-start | bytes 6148
Sparse Core Ops, SparseCore 0:
  13.9 129.3 all-gather.2
  146.6 83.9 all-gather.4
Sparse Core Ops, SparseCore 1:
  184.1 50.4 reduce-scatter.4
  326.1 25.1 reduce-scatter.2
